TPU v7x, 32 devices: a whole 2x2x4 slice. The times are simulated.
32 devices in a mesh: ep: 8 (over z, core), tp: 4 (over y, x).
Axes of the slice: x: 2, y: 2, z: 4, core: 2. Of those that a mesh axis runs over, the one named last changes fastest.
Arguments:
- query_rows: bfloat16 [4096, 2048], P('ep', 'tp'), may hold values from -6 to 6
- key_rows: bfloat16 [4096, 2048], P('ep', 'tp'), may hold values from -6 to 6
- value_rows: bfloat16 [4096, 4096], P('ep', 'tp'), may hold values from -6 to 6
- in_gate: float32 [16, 4096], P('tp', 'ep'), may hold values from -120 to 120
- forget_gate: float32 [16, 4096], P('tp', 'ep'), may hold values from -2 to 20
- out_gate: bfloat16 [4096, 4096], P('ep', 'tp'), may hold values from -6 to 6
- head_gain: float32 [4096], P('tp'), may hold values from 0.1 to 1.9
- mix_weight: bfloat16 [4096, 4096], P(None, 'tp'), may hold values from -0.09375 to 0.09375
- expert_input: bfloat16 [2048, 4096], P('ep', 'tp'), may hold values from -30 to 30
- routes: int32 [2048, 2], P('ep'), may hold values from 0 to 7, all different within a row; in each aligned block of 256 rows (0 to 255, 256 to 511, ...) at most 128 rows name the same one
- route_weight: float32 [2048, 2], P('ep'), may hold values from 0.25 to 1.25
- gate_weight: bfloat16 [8, 1024, 4096], P('ep', 'tp'), may hold values from -0.09375 to 0.09375
- up_weight: bfloat16 [8, 1024, 4096], P('ep', 'tp'), may hold values from -0.09375 to 0.09375
- down_weight: bfloat16 [8, 1024, 4096], P('ep', None, 'tp'), may hold values from -0.1875 to 0.1875
Outputs:
- mixer_out: bfloat16 [4096, 4096], P('ep', 'tp')
- expert_out: bfloat16 [2048, 4096], P('ep', 'tp')
Inputs may be any that keep to these rules, and one draw needn't show every extreme that they name: `routes`: each row names 2 different experts. In the rows of one device no expert is named by more than 128 rows, and in the rows of some device an expert is named by exactly 128 rows.
All inputs are finite; a program needn't handle non-finite values.
Results may differ from a plain program's by a relative error of at most 0.0057.
Values may be sent and summed in bfloat16 or wider, within the bound.
No kernel may reach another device: no remote copies, remote signals or barrier semaphores. Data moves between devices by JAX's collectives and lax.ppermute only.
A program may use at most 128 MiB of HBM per device.

v0:
```python
import jax
import jax.numpy as jnp
from jax import lax
from jax.sharding import PartitionSpec as P

D = 4096
BLOCK = 64
EPSILON = 1e-06
LOG_FLOOR = -1e30
HIGHEST_PRECISION = lax.Precision.HIGHEST


def carried_in(value, axis, join, neutral):
    count, mine = (lax.axis_size(axis), lax.axis_index(axis))
    pieces = jax.tree.map(lambda part: lax.all_gather(part, axis), value)
    subtotal = jax.tree.map(
        lambda part, zero: jnp.full_like(part, 0) + jnp.asarray(zero, part.dtype), value, neutral
    )

    def turn(position, subtotal):
        longer = join(subtotal, jax.tree.map(lambda part: part[position], pieces))
        return jax.tree.map(lambda new, old: jnp.where(position < mine, new, old), longer, subtotal)

    return lax.fori_loop(0, count - 1, turn, subtotal)


def combine(first_part, second_part):
    decay_first, max_first, memory_first, normal_first = first_part
    decay_second, max_second, memory_second, normal_second = second_part
    running_max = jnp.maximum(decay_second + max_first, max_second)
    keep_first = jnp.exp(decay_second + max_first - running_max)
    keep_second = jnp.exp(max_second - running_max)
    memory = (
        keep_first[..., None, None] * memory_first + keep_second[..., None, None] * memory_second
    )
    normalizer = keep_first[..., None] * normal_first + keep_second[..., None] * normal_second
    return (decay_first + decay_second, running_max, memory, normalizer)


def identity_state(head_count, key_width, value_width):
    return (
        jnp.zeros((head_count,), jnp.float32),
        jnp.full((head_count,), LOG_FLOOR, jnp.float32),
        jnp.zeros((head_count, key_width, value_width), jnp.float32),
        jnp.zeros((head_count, key_width), jnp.float32),
    )


def halfprod(form, left, right):
    return jnp.einsum(form, left, right, preferred_element_type=jnp.float32)


def prepare(query_heads, key_heads, value_heads, in_gate, forget_gate):
    head_count, length, key_width = query_heads.shape
    block_count = length // BLOCK
    query_blocks = query_heads.reshape(head_count, block_count, BLOCK, key_width)
    key_blocks = key_heads.reshape(head_count, block_count, BLOCK, key_width)
    value_blocks = value_heads.reshape(head_count, block_count, BLOCK, value_heads.shape[-1])
    log_input = in_gate.reshape(head_count, block_count, BLOCK)
    cumulative = jnp.cumsum(
        jax.nn.log_sigmoid(forget_gate).reshape(head_count, block_count, BLOCK), axis=-1
    )
    block_decay = cumulative[..., -1]
    weight_log = block_decay[..., None] - cumulative + log_input
    block_max = jnp.max(weight_log, axis=-1)
    weighted = (
        key_blocks.astype(jnp.float32) * jnp.exp(weight_log - block_max[..., None])[..., None]
    )
    normalizer = jnp.sum(weighted, axis=2)
    memory = halfprod("hcsk,hcsv->hckv", weighted.astype(jnp.bfloat16), value_blocks)
    return (
        (query_blocks, key_blocks, value_blocks, log_input, cumulative),
        (block_decay, block_max, memory, normalizer),
    )


def prefix(summary, initial):
    leading = jax.tree.map(lambda tensor: jnp.moveaxis(tensor, 1, 0), summary)

    def advance(running, current):
        return (combine(running, current), running)

    final_state, before = lax.scan(advance, initial, leading)
    return (final_state, jax.tree.map(lambda tensor: jnp.moveaxis(tensor, 0, 1), before))


def block_outputs(blocked, before):
    query_blocks, key_blocks, value_blocks, log_input, cumulative = blocked
    prior_max, prior_memory, prior_normal = (before[1], before[2], before[3])
    block_len = cumulative.shape[-1]
    scale = query_blocks.shape[-1] ** (-0.5)
    causal = jnp.tril(jnp.ones((block_len, block_len), dtype=bool))
    log_decay = jnp.where(
        causal,
        cumulative[..., :, None] - cumulative[..., None, :] + log_input[..., None, :],
        -jnp.inf,
    )
    log_inter = cumulative + prior_max[..., None]
    top_value = jnp.maximum(log_inter, jnp.max(log_decay, axis=-1))
    scores = (
        halfprod("hctk,hcsk->hcts", query_blocks, key_blocks)
        * scale
        * jnp.exp(log_decay - top_value[..., None])
    )
    carried = jnp.exp(log_inter - top_value) * scale
    query_wide = query_blocks.astype(jnp.float32)
    numerator = carried[..., None] * jnp.einsum(
        "hctk,hckv->hctv", query_wide, prior_memory, precision=HIGHEST_PRECISION
    ) + halfprod("hcts,hcsv->hctv", scores.astype(jnp.bfloat16), value_blocks)
    denominator = carried * jnp.einsum(
        "hctk,hck->hct", query_wide, prior_normal, precision=HIGHEST_PRECISION
    ) + jnp.sum(scores, axis=-1)
    return numerator / jnp.maximum(jnp.abs(denominator), jnp.exp(-top_value))[..., None]


def finish(head_values, out_gate, head_gain):
    head_count, block_count, block_len, value_width = head_values.shape
    per_head = jnp.transpose(head_values, (1, 2, 0, 3)).reshape(
        block_count * block_len, head_count, value_width
    )
    per_head = per_head * lax.rsqrt(jnp.mean(per_head * per_head, axis=-1, keepdims=True) + EPSILON)
    per_head = per_head.reshape(block_count * block_len, head_count * value_width) * head_gain
    per_head = per_head * jax.nn.sigmoid(out_gate.astype(jnp.float32))
    return per_head.astype(jnp.bfloat16)


def cell_heads(query_rows, key_rows, value_rows, in_gate, forget_gate, out_gate, head_gain):
    length = query_rows.shape[0]
    head_count = in_gate.shape[0]
    key_width = query_rows.shape[1] // head_count
    value_width = value_rows.shape[1] // head_count
    query_heads = query_rows.reshape(length, head_count, key_width).transpose(1, 0, 2)
    key_heads = key_rows.reshape(length, head_count, key_width).transpose(1, 0, 2)
    value_heads = value_rows.reshape(length, head_count, value_width).transpose(1, 0, 2)
    blocked, summary = prepare(query_heads, key_heads, value_heads, in_gate, forget_gate)
    initial = identity_state(head_count, key_width, value_width)
    final_state, before = prefix(summary, initial)
    incoming = carried_in(final_state, "ep", combine, initial)
    expanded = jax.tree.map(lambda tensor: tensor[:, None], incoming)
    before = combine(expanded, before)
    return finish(block_outputs(blocked, before), out_gate, head_gain)


def body(
    query_rows,
    key_rows,
    value_rows,
    in_gate,
    forget_gate,
    out_gate,
    head_gain,
    mix_weight,
    expert_input,
    routes,
    route_weight,
    gate_weight,
    up_weight,
    down_weight,
):
    mixed_heads = cell_heads(
        query_rows, key_rows, value_rows, in_gate, forget_gate, out_gate, head_gain
    )
    gate_local = gate_weight[0]
    up_local = up_weight[0]
    down_local = down_weight[0]
    group_size = lax.axis_size("ep")
    token_count, fanout = routes.shape
    capacity = 2 * token_count * fanout // group_size
    slot_count = group_size * capacity
    chosen = routes.reshape(-1)
    one_hot = (chosen[:, None] == jnp.arange(group_size, dtype=jnp.int32)[None, :]).astype(
        jnp.int32
    )
    position = jnp.sum((jnp.cumsum(one_hot, axis=0) - one_hot) * one_hot, axis=1)
    target = chosen * capacity + position
    matches = (jnp.arange(slot_count, dtype=jnp.int32)[:, None] == target[None, :]).astype(
        jnp.int32
    )
    occupied = jnp.sum(matches, axis=1) > 0
    source_row = jnp.sum(
        matches * (jnp.arange(token_count * fanout, dtype=jnp.int32) // fanout)[None, :], axis=1
    )
    arrived = lax.all_to_all(
        jnp.where(
            occupied[:, None],
            jnp.take(expert_input, source_row, axis=0),
            jnp.zeros((), expert_input.dtype),
        ),
        "ep",
        split_axis=0,
        concat_axis=0,
        tiled=True,
    )
    head_piece = lax.all_gather(mixed_heads, "tp", axis=1, tiled=True)
    token_piece = lax.all_gather(arrived, "tp", axis=1, tiled=True)
    mix_acc = jnp.dot(head_piece, mix_weight, preferred_element_type=jnp.float32)
    gate_acc = jnp.einsum("sd,fd->sf", token_piece, gate_local, preferred_element_type=jnp.float32)
    up_acc = jnp.einsum("sd,fd->sf", token_piece, up_local, preferred_element_type=jnp.float32)
    squares = jnp.sum(jnp.square(token_piece.astype(jnp.float32)), axis=1)
    mix_acc, gate_acc, up_acc, squares = (mix_acc, gate_acc, up_acc, squares)
    mixer_out = mix_acc.astype(jnp.bfloat16)
    inverse_rms = lax.rsqrt(squares / D + EPSILON)[:, None]
    hidden = (jax.nn.silu(gate_acc * inverse_rms) * (up_acc * inverse_rms)).astype(jnp.bfloat16)
    expert_rows = jnp.dot(
        lax.all_gather(hidden, "tp", axis=1, tiled=True),
        down_local,
        preferred_element_type=jnp.float32,
    )
    returned_rows = lax.all_to_all(
        expert_rows.astype(jnp.bfloat16), "ep", split_axis=0, concat_axis=0, tiled=True
    )
    picked_rows = (
        jnp.take(returned_rows, target, axis=0).reshape(token_count, fanout, -1).astype(jnp.float32)
    )
    expert_out = jnp.sum(picked_rows * route_weight[:, :, None], axis=1).astype(jnp.bfloat16)
    return (mixer_out, expert_out)


def solution(mesh):
    in_specs = (
        P("ep", "tp"),
        P("ep", "tp"),
        P("ep", "tp"),
        P("tp", "ep"),
        P("tp", "ep"),
        P("ep", "tp"),
        P("tp"),
        P(None, "tp"),
        P("ep", "tp"),
        P("ep", None),
        P("ep", None),
        P("ep", "tp", None),
        P("ep", "tp", None),
        P("ep", None, "tp"),
    )
    out_specs = (P("ep", "tp"), P("ep", "tp"))
    return jax.shard_map(body, mesh=mesh, in_specs=in_specs, out_specs=out_specs, check_vma=False)
```

profile of v0, /device:TPU:0, one launch (start us, length us, event | category | flops | bytes accessed | tf_op | source)
XLA Modules:
  0.0 351.7 jit_solution(7868608144681176539)
XLA Ops:
  7.3 0.8 fusion.56
  8.2 0.8 reshape.226
  9.0 0.9 reduce_window_sum.28
  10.5 2.6 reshape.229
  13.1 2.3 copy.78
  15.4 1.2 reshape.227
  17.1 1.0 copy-done.5
  18.0 3.1 convolution_bitcast_fusion
  21.1 18.0 %while.43 = (s32[]{:T(128)}, f32[4]{0:T(128)S(1)}, f32[4]{0:T(128)S(1)}, f32[4,128,256]{2,1,0:T(8,128)S(1)}, f32[4,128]{1,0:T(4,128)S(1)}, /*index=5*/f32[8,4]{1...) while((s32[]{:T(128)}, f32[4]{0:T(128)S(1)}, ...), condition=%wide.region_4.5_spmd.clone, body=%wide.region_3.4_spmd.clone.sunk | while | flops 657951 | bytes 2636291 | solution.py:83
  21.1 0.9 bitcast_dynamic-update-slice_fusion.4
  22.0 1.2 fusion.83
  23.4 0.9 bitcast_dynamic-update-slice_fusion.4
  24.3 1.2 fusion.83
  25.7 0.8 bitcast_dynamic-update-slice_fusion.4
  26.5 1.2 fusion.83
  27.9 0.8 bitcast_dynamic-update-slice_fusion.4
  28.8 1.2 fusion.83
  30.2 0.9 bitcast_dynamic-update-slice_fusion.4
  31.1 1.2 fusion.83
  32.4 0.9 bitcast_dynamic-update-slice_fusion.4
  33.3 1.2 fusion.83
  34.7 0.8 bitcast_dynamic-update-slice_fusion.4
  35.5 1.2 fusion.83
  36.9 0.8 bitcast_dynamic-update-slice_fusion.4
  37.8 1.2 fusion.83
  39.2 0.8 copy-done.2
  40.5 1.1 reduce-window.6
  42.0 0.6 convert_reduce_fusion
  42.6 5.4 %gather_fusion = bf16[1024,1024]{1,0:T(8,128)(2,1)} fusion(bf16[256,1024]{1,0:T(8,128)(2,1)S(1)} %copy-done.1, s32[1024]{0:T(1024)S(1)} %broadcast_clamp_fusion), kind=kCustom, calls=%fused_computation | custom fusion | bytes 4198400 | tf_op jit(solution)/shard_map/jit(_take)/gather | solution.py:186
  48.0 1.9 select_select_fusion
  49.9 83.4 %all_to_all.21 = bf16[8,128,1024]{2,1,0:T(8,128)(2,1)} all-to-all(bf16[8,128,1024]{2,1,0:T(8,128)(2,1)S(1)} %select_select_fusion), channel_id=1, replica_groups=mesh['ep'=8,'tp'=4] {'ep'}, dimensions={0} | all-to-all | bytes 4194304 | tf_op jit(solution)/shard_map/all_to_all | solution.py:183
  135.6 14.3 %all-reduce.2 = (f32[32]{0:T(128)S(1)}, f32[32]{0:T(128)S(1)}) all-reduce(f32[32]{0:T(128)S(1)} %dynamic-update-slice, f32[32]{0:T(128)S(1)} %dynamic-update-slice.1), channel_id=2, replica_groups=mesh['ep'=8,'tp'=4] {'ep'}, use_global_device_ids=true, to_apply=%add | all-reduce | flops 64 | bytes 512
  150.0 0.9 reshape.231
  151.0 1.1 copy.84
  152.1 13.0 %all-gather.4 = f32[8,4,128]{2,1,0:T(4,128)S(1)} all-gather(f32[1,4,128]{2,1,0:T(4,128)S(1)} %bitcast.238), channel_id=5, replica_groups=mesh['ep'=8,'tp'=4] {'ep'}, dimensions={0}, use_global_device_ids=true | all-gather | bytes 18432 | tf_op jit(solution)/shard_map/all_gather | solution.py:15
  165.0 0.6 fusion.41
  165.7 9.6 %while.44 = (s32[]{:T(128)}, f32[4]{0:T(128)S(1)}, f32[4,128,256]{2,1,0:T(8,128)S(1)}, f32[4,128]{1,0:T(4,128)S(1)}, s32[]{:T(128)}, /*index=5*/f32[8,4]{1,0:T(8...) while((s32[]{:T(128)}, f32[4]{0:T(128)S(1)}, ...), condition=%wide.region_6.7_spmd.clone, body=%wide.region_5.6_spmd.clone.sunk | while | flops 657956 | bytes 1579390 | solution.py:24
  165.8 1.2 fusion.84
  167.1 1.2 fusion.84
  168.4 1.2 fusion.84
  169.8 1.2 fusion.84
  171.1 1.2 fusion.84
  172.4 1.3 fusion.84
  173.9 1.3 fusion.84
  175.4 44.2 %all-gather.12.cloned.1.call-done = bf16[1024,4096]{1,0:T(8,128)(2,1)} async-done(((bf16[1024,1024]{1,0:T(8,128)(2,1)}), bf16[1024,4096]{1,0:T(8,128)(2,1)}) %all-gather.12.cloned.1.call-update) | async-done | bytes 8388624 | tf_op jit(solution)/shard_map/all_gather | solution.py:195
  219.6 5.2 %multiply_reduce_fusion = f32[1024]{0:T(1024)S(1)} fusion(bf16[1024,4096]{1,0:T(8,128)(2,1)} %all-gather.12.cloned.1.call-done), kind=kLoop, calls=%fused_computation.36 | loop fusion | flops 12581888 | bytes 8392704 | tf_op jit(solution)/shard_map/reduce_sum | solution.py:199
  225.4 4.1 %fusion.29 = f32[1024,256]{1,0:T(8,128)S(1)} fusion(bf16[1024,4096]{1,0:T(8,128)(2,1)S(1)} %copy-done.3, bf16[1,256,4096]{2,1,0:T(8,128)(2,1)} %param.29, f32[1024]{0:T(1024)S(1)} %add_rsqrt_fusion.1), kind=kOutput, calls=%fused_computation.63 | convolution fusion | flops 2147745792 | bytes 11538432 | tf_op jit(solution)/shard_map/sd,fd->sf/dot_general | solution.py:197
  229.5 3.3 fusion.38
  233.3 0.9 fusion.53
  234.2 1.7 fusion.65
  236.0 4.4 %fusion.16 = f32[4,8,256,64]{2,3,1,0:T(8,128)S(1)} fusion(bf16[4,8,64,128]{3,2,1,0:T(8,128)(2,1)S(1)} %bitcast.231, f32[8,4,128,256]{3,2,1,0:T(8,128)} %get-tuple-element.240, f32[4,8]{0,1:T(8,128)S(1)} %fusion.58, f32[4,128,256]{2,1,0:T(8,128)S(1)} %get-tuple-element.239, f32[4,8]{0,1:T(8,128)S(1)} %get-tuple-element.432), kind=kOutput, calls=%fused_computation.39 | convolution fusion | flops 808452096 | bytes 7340288 | tf_op jit(solution)/shard_map/hctk,hckv->hctv/dot_general | solution.py:107
  240.4 1.6 multiply_reduce_fusion.2
  242.1 1.4 copy.88
  243.5 1.8 copy.102
  246.6 1.1 copy-done.4
  247.9 1.6 multiply_convert_fusion
  249.6 18.4 %all-gather.14.cloned.1.call-done = bf16[1024,1024]{1,0:T(8,128)(2,1)} async-done(((bf16[1024,256]{1,0:T(8,128)(2,1)}), bf16[1024,1024]{1,0:T(8,128)(2,1)}) %all-gather.14.cloned.1.call-update) | async-done | bytes 2097168 | tf_op jit(solution)/shard_map/all_gather | solution.py:205
  268.0 5.3 %fusion.25 = bf16[1024,1024]{1,0:T(8,128)(2,1)} fusion(bf16[1024,1024]{1,0:T(8,128)(2,1)} %all-gather.14.cloned.1.call-done, bf16[1,1024,1024]{2,1,0:T(8,128)(2,1)S(1)} %copy-done), kind=kOutput, calls=%fused_computation.59 | convolution fusion | flops 2148532224 | bytes 6291456 | tf_op jit(solution)/shard_map/dot_general | solution.py:204
  273.3 4.7 %all-to-all-start.1 = ((bf16[8,128,1024]{2,1,0:T(8,128)(2,1)}), bf16[8,128,1024]{2,1,0:T(8,128)(2,1)}, u32[]{:S(2)}, u32[]{:S(2)}) async-start(bf16[8,128,1024]{2,1,0:T(8,128)(2,1)} %bitcast.232), calls=%async_computation.1 | async-start | bytes 4194304 | tf_op jit(solution)/shard_map/all_to_all | solution.py:209
  278.9 44.0 %all-gather.10.cloned.1.call-done = bf16[512,4096]{1,0:T(8,128)(2,1)} async-done(((bf16[512,1024]{1,0:T(8,128)(2,1)}), bf16[512,4096]{1,0:T(8,128)(2,1)}) %all-gather.10.cloned.1.call-update) | async-done | bytes 4194320 | tf_op jit(solution)/shard_map/all_gather | solution.py:194
  322.9 10.1 %convolution_convert_fusion = bf16[512,1024]{1,0:T(8,128)(2,1)} fusion(bf16[512,4096]{1,0:T(8,128)(2,1)} %all-gather.10.cloned.1.call-done, bf16[4096,1024]{1,0:T(8,128)(2,1)} %param.25), kind=kOutput, calls=%fused_computation.60 | convolution fusion | flops 4295491584 | bytes 13631488 | tf_op jit(solution)/shard_map/dot_general | solution.py:196
  333.0 4.6 %gather_fusion.1 = bf16[512,1024]{1,0:T(8,128)(2,1)S(1)} fusion(bf16[1024,1024]{1,0:T(8,128)(2,1)} %bitcast.39, s32[1024]{0:T(1024)S(1)} %pad_clamp_fusion), kind=kCustom, calls=%fused_computation.1 | custom fusion | bytes 2099200 | tf_op jit(solution)/shard_map/jit(_take)/gather | solution.py:213
  337.6 1.2 gather.15
  338.8 6.3 %multiply_reduce_fusion.1 = bf16[256,1024]{1,0:T(8,128)(2,1)} fusion(bf16[256,2,1024]{2,1,0:T(2,128)(2,1)} %gather.15, pred[256,2]{1,0:T(8,128)(4,1)S(1)} %copy.93, f32[256,2]{1,0:T(8,128)S(1)} %copy.95), kind=kLoop, calls=%fused_computation.51 | loop fusion | flops 1835008 | bytes 1575424 | tf_op jit(solution)/shard_map/reduce_sum | solution.py:215
  (177 shorter events, 9.8 us)
Async XLA Ops:
  7.2 260.8 %copy-start = (bf16[1,1024,1024]{2,1,0:T(8,128)(2,1)S(1)}, bf16[1,1024,1024]{2,1,0:T(8,128)(2,1)}, u32[]{:S(2)}) copy-start(bf16[1,1024,1024]{2,1,0:T(8,128)(2,1)} %param.31) | copy-start | bytes 6291460
  7.2 158.5 %all-gather.16.cloned.1.call-start = ((), (), s32[]{:S(2)}) async-start(), calls=%async_computation.5 | async-start | bytes 4718592 | tf_op jit(solution)/shard_map/all_gather | solution.py:15
  16.6 1.4 copy-start.5
  16.7 4.4 %copy-start.7 = (bf16[4,512,128]{2,1,0:T(8,128)(2,1)}, bf16[4,512,128]{2,1,0:T(8,128)(2,1)S(1)}, u32[]{:S(2)}) copy-start(bf16[4,512,128]{2,1,0:T(8,128)(2,1)S(1)} %copy.77) | copy-start | bytes 1572868
  21.1 18.9 %copy-start.10 = (s32[256,2]{0,1:T(2,128)S(1)}, s32[256,2]{0,1:T(2,128)}, u32[]{:S(2)}) copy-start(s32[256,2]{0,1:T(2,128)} %param.27) | copy-start | bytes 6148
  39.1 0.8 copy-start.2
  39.2 3.5 copy-start.1
  40.0 179.6 %all-gather.12.cloned.1.call-start = ((), (), s32[]{:S(2)}) async-start(), calls=%async_computation.3 | async-start | bytes 10485760 | tf_op jit(solution)/shard_map/all_gather | solution.py:195
  133.2 0.7 copy-start.14
  133.2 16.8 %copy-start.9 = (bf16[512,512]{1,0:T(8,128)(2,1)S(1)}, bf16[512,512]{1,0:T(8,128)(2,1)}, u32[]{:S(2)}) copy-start(bf16[512,512]{1,0:T(8,128)(2,1)} %param.18) | copy-start | bytes 1572868
  133.3 134.7 %all-gather.14.cloned.1.call-start = ((), (), s32[]{:S(2)}) async-start(), calls=%async_computation.4 | async-start | bytes 2621440 | tf_op jit(solution)/shard_map/all_gather | solution.py:205
  219.6 5.8 %copy-start.3 = (bf16[1024,4096]{1,0:T(8,128)(2,1)S(1)}, bf16[1024,4096]{1,0:T(8,128)(2,1)}, u32[]{:S(2)}) copy-start(bf16[1024,4096]{1,0:T(8,128)(2,1)} %all-gather.12.cloned.1.call-done) | copy-start | bytes 25165828
  225.4 4.1 %copy-start.13 = (bf16[1,256,4096]{2,1,0:T(8,128)(2,1)S(1)}, bf16[1,256,4096]{2,1,0:T(8,128)(2,1)}, u32[]{:S(2)}) copy-start(bf16[1,256,4096]{2,1,0:T(8,128)(2,1)} %param.30) | copy-start | bytes 6291460
  232.8 90.1 %all-gather.10.cloned.1.call-start = ((), (), s32[]{:S(2)}) async-start(), calls=%async_computation.2 | async-start | bytes 5242880 | tf_op jit(solution)/shard_map/all_gather | solution.py:194
  236.0 4.4 %copy-start.6 = (bf16[4,512,256]{2,1,0:T(8,128)(2,1)S(1)}, bf16[4,512,256]{2,1,0:T(8,128)(2,1)}, u32[]{:S(2)}) copy-start(bf16[4,512,256]{2,1,0:T(8,128)(2,1)} %copy.78) | copy-start | bytes 3145732
  246.1 1.6 copy-start.4
  246.1 1.8 copy-start.8
  246.1 1.8 copy-start.11
  273.3 5.5 %copy-start.12 = (f32[256,2]{0,1:T(2,128)S(1)}, f32[256,2]{0,1:T(2,128)}, u32[]{:S(2)}) copy-start(f32[256,2]{0,1:T(2,128)} %param.28) | copy-start | bytes 6148
  273.3 59.7 %all-to-all-start.1 = ((bf16[8,128,1024]{2,1,0:T(8,128)(2,1)}), bf16[8,128,1024]{2,1,0:T(8,128)(2,1)}, u32[]{:S(2)}, u32[]{:S(2)}) async-start(bf16[8,128,1024]{2,1,0:T(8,128)(2,1)} %bitcast.232), calls=%async_computation.1 | async-start | bytes 4194304 | tf_op jit(solution)/shard_map/all_to_all | solution.py:209
Sparse Core Ops, SparseCore 0:
  40.1 86.1 all-gather.15
  133.4 86.1 all-gather.11
  232.9 35.0 all-gather.13
  270.3 52.5 all-gather.9
where the time goes:
time: 353 us; the launch traced here: 352 us
  blocking collectives  111 us (31%)
  waiting for transfers between devices  107 us (30%)
  other arithmetic  47 us (13%)
  matrix products  34.5 us (10%)
  local copies, waits for them, and re-layouts  32.5 us (9%)
  between operations  14.9 us (4%)
  starting transfers between devices  5.12 us (1%)
    all_to_all x1, blocking collectives, body(): lax.all_to_all(jnp.where(occupied[:, None], jnp.take(expert_input, source...  83.4 us
    all_gather x1, waiting for transfers between devices, body(): token_piece = lax.all_gather(arrived, 'tp', axis=1, tiled=True)  44.2 us
    all_gather x1, waiting for transfers between devices, body(): head_piece = lax.all_gather(mixed_heads, 'tp', axis=1, tiled=True)  44 us
    all_gather x1, waiting for transfers between devices, body(): lax.all_gather(hidden, 'tp', axis=1, tiled=True)  18.4 us
    unnamed x1, blocking collectives  14.3 us
    all_gather x1, blocking collectives, carried_in(): pieces = jax.tree.map(lambda part: lax.all_gather(part, axis), value)  13 us
    dot_general x1, matrix products, body(): jnp.dot(head_piece, mix_weight, preferred_element_type=jnp.float32)  10.1 us
    add x8, other arithmetic, combine(): keep_first[..., None, None] * memory_first  9.38 us
  transfers between devices with their start and end apart: 5, of which 3 were waited for; matrix products, arithmetic and copies ran while one was open for 16% of the time, Pallas kernels for 0%

commit v1 on v0

--- a/solution.py
+++ b/solution.py
@@ -191,8 +191,13 @@
         concat_axis=0,
         tiled=True,
     )
-    head_piece = lax.all_gather(mixed_heads, "tp", axis=1, tiled=True)
-    token_piece = lax.all_gather(arrived, "tp", axis=1, tiled=True)
+    head_piece, token_piece = jnp.split(
+        lax.all_gather(
+            jnp.concatenate([mixed_heads, arrived], 0), axis_name="tp", axis=1, tiled=True
+        ),
+        [mixed_heads.shape[0]],
+        0,
+    )
     mix_acc = jnp.dot(head_piece, mix_weight, preferred_element_type=jnp.float32)
     gate_acc = jnp.einsum("sd,fd->sf", token_piece, gate_local, preferred_element_type=jnp.float32)
     up_acc = jnp.einsum("sd,fd->sf", token_piece, up_local, preferred_element_type=jnp.float32)

time: 353 us -> 434 us (1.23)
  waiting for transfers between devices: 107 us -> 194 us
  blocking collectives: 111 us -> 91.9 us
  starting transfers between devices: 5.12 us -> 11.6 us
    all_to_all x1 -> x0, blocking collectives: 83.4 us -> none  [body(): lax.all_to_all(jnp.where(occupied[:, None], jnp.take(expert_input, source...]
    unnamed x1, blocking collectives: 14.3 us -> 71.1 us
    all_to_all x1, waiting for transfers between devices: 0.01 us -> 38.1 us  [body(): lax.all_to_all(expert_rows.astype(jnp.bfloat16), 'ep', split_axis=0, conc...]
    all_gather x2 -> x1, waiting for transfers between devices: 88.1 us -> 121 us  [body(): lax.all_gather(jnp.concatenate([mixed_heads, arrived], 0), axis_name='tp'...]
    all_gather x1, waiting for transfers between devices: 18.4 us -> 35.2 us  [body(): lax.all_gather(hidden, 'tp', axis=1, tiled=True)]
    all_gather x1, blocking collectives: 13 us -> 20.8 us  [carried_in(): pieces = jax.tree.map(lambda part: lax.all_gather(part, axis), value)]
    all_to_all x0 -> x1, starting transfers between devices: none -> 6.55 us  [body(): lax.all_to_all(jnp.where(occupied[:, None], jnp.take(expert_input, source...]
  transfers between devices with their start and end apart: 5 -> 5, of which waited for: 3 -> 3; matrix products, arithmetic and copies ran while one was open for 16% -> 11% of each run, Pallas kernels for 0% -> 0%
where the time goes in v1:
time: 434 us; the launch traced here: 433 us
  waiting for transfers between devices  194 us (45%)
  blocking collectives  91.9 us (21%)
  other arithmetic  50.2 us (12%)
  matrix products  38.3 us (9%)
  local copies, waits for them, and re-layouts  31 us (7%)
  between operations  14.9 us (3%)
  starting transfers between devices  11.6 us (3%)
    all_gather x1, waiting for transfers between devices, body(): lax.all_gather(jnp.concatenate([mixed_heads, arrived], 0), axis_name='tp'...  121 us
    unnamed x1, blocking collectives  71.1 us
    all_to_all x1, waiting for transfers between devices, body(): lax.all_to_all(expert_rows.astype(jnp.bfloat16), 'ep', split_axis=0, conc...  38.1 us
    all_gather x1, waiting for transfers between devices, body(): lax.all_gather(hidden, 'tp', axis=1, tiled=True)  35.2 us
    all_gather x1, blocking collectives, carried_in(): pieces = jax.tree.map(lambda part: lax.all_gather(part, axis), value)  20.8 us
    dot_general x1, matrix products, body(): jnp.dot(head_piece, mix_weight, preferred_element_type=jnp.float32)  10.1 us
    add x8, other arithmetic, combine(): keep_first[..., None, None] * memory_first  9.34 us
    select_n x14, other arithmetic, turn(): jnp.where(position < mine, new, old)  8.95 us
  transfers between devices with their start and end apart: 5, of which 3 were waited for; matrix products, arithmetic and copies ran while one was open for 11% of the time, Pallas kernels for 0%

profile of v1, /device:TPU:0, one launch (start us, length us, event | category | flops | bytes accessed | tf_op | source)
XLA Modules:
  0.0 432.6 jit_solution(13197494657384588470)
XLA Ops:
  7.3 0.8 fusion.71
  8.2 0.9 reduce_window_sum.28
  9.3 0.8 reshape.226
  10.3 1.2 reshape.227
  11.5 0.9 copy.77
  12.3 2.6 reshape.229
  15.0 2.4 copy.78
  17.9 4.5 %convolution_bitcast_fusion = f32[8,4,128,256]{3,2,0,1:T(8,128)} fusion(bf16[4,8,64,256]{3,2,1,0:T(8,128)(2,1)} %bitcast.225, bf16[4,8,64,128]{3,2,1,0:T(8,128)(2,1)} %bitcast.232, f32[4,8,64]{2,1,0:T(8,128)S(1)} %subtract_exponential_fusion.4), kind=kOutput, calls=%fused_computation.48 | convolution fusion | flops 135004160 | bytes 5775360 | tf_op jit(solution)/shard_map/hcsk,hcsv->hckv/dot_general | solution.py:50
  22.4 18.1 %while.43 = (s32[]{:T(128)}, f32[4]{0:T(128)S(1)}, f32[4]{0:T(128)S(1)}, f32[4,128,256]{2,1,0:T(8,128)S(1)}, f32[4,128]{1,0:T(4,128)S(1)}, /*index=5*/f32[8,4]{1...) while((s32[]{:T(128)}, f32[4]{0:T(128)S(1)}, ...), condition=%wide.region_4.5_spmd.clone, body=%wide.region_3.4_spmd.clone.sunk | while | flops 657951 | bytes 2636791 | solution.py:83
  22.4 0.8 bitcast_dynamic-update-slice_fusion.4
  23.3 1.2 fusion.95
  24.7 0.9 bitcast_dynamic-update-slice_fusion.4
  25.5 1.2 fusion.95
  26.9 0.9 bitcast_dynamic-update-slice_fusion.4
  27.8 1.2 fusion.95
  29.2 0.9 bitcast_dynamic-update-slice_fusion.4
  30.1 1.2 fusion.95
  31.5 0.9 bitcast_dynamic-update-slice_fusion.4
  32.3 1.2 fusion.95
  33.7 0.9 bitcast_dynamic-update-slice_fusion.4
  34.6 1.2 fusion.95
  36.0 0.8 bitcast_dynamic-update-slice_fusion.4
  36.8 1.2 fusion.95
  38.2 0.9 bitcast_dynamic-update-slice_fusion.4
  39.1 1.2 fusion.95
  40.5 0.8 copy-done.2
  41.7 1.1 reduce-window.6
  43.9 5.4 %gather_fusion = bf16[1024,1024]{1,0:T(8,128)(2,1)} fusion(bf16[256,1024]{1,0:T(8,128)(2,1)S(1)} %copy-done.1, s32[1024]{0:T(1024)S(1)} %broadcast_clamp_fusion), kind=kCustom, calls=%fused_computation | custom fusion | bytes 4198400 | tf_op jit(solution)/shard_map/jit(_take)/gather | solution.py:186
  49.3 2.8 select_select_fusion
  52.1 6.5 %all-to-all-start = ((bf16[8,128,1024]{2,1,0:T(8,128)(2,1)}), bf16[8,128,1024]{2,1,0:T(8,128)(2,1)}, u32[]{:S(2)}, u32[]{:S(2)}) async-start(bf16[8,128,1024]{2,1,0:T(8,128)(2,1)} %select_select_fusion), calls=%async_computation | async-start | bytes 4194304 | tf_op jit(solution)/shard_map/all_to_all | solution.py:183
  60.4 71.1 %all-reduce.2 = (f32[32]{0:T(128)S(1)}, f32[32]{0:T(128)S(1)}) all-reduce(f32[32]{0:T(128)S(1)} %dynamic-update-slice, f32[32]{0:T(128)S(1)} %dynamic-update-slice.1), channel_id=2, replica_groups=mesh['ep'=8,'tp'=4] {'ep'}, use_global_device_ids=true, to_apply=%add | all-reduce | flops 64 | bytes 512
  131.7 0.9 reshape.231
  132.6 1.1 copy.84
  133.7 20.8 %all-gather.4 = f32[8,4,128]{2,1,0:T(4,128)S(1)} all-gather(f32[1,4,128]{2,1,0:T(4,128)S(1)} %bitcast.236), channel_id=5, replica_groups=mesh['ep'=8,'tp'=4] {'ep'}, dimensions={0}, use_global_device_ids=true | all-gather | bytes 18432 | tf_op jit(solution)/shard_map/all_gather | solution.py:15
  154.5 0.6 fusion.56
  155.2 9.3 %while.44 = (s32[]{:T(128)}, f32[4]{0:T(128)S(1)}, f32[4,128,256]{2,1,0:T(8,128)S(1)}, f32[4,128]{1,0:T(4,128)S(1)}, s32[]{:T(128)}, /*index=5*/f32[8,4]{1,0:T(8...) while((s32[]{:T(128)}, f32[4]{0:T(128)S(1)}, ...), condition=%wide.region_6.7_spmd.clone, body=%wide.region_5.6_spmd.clone.sunk | while | flops 657956 | bytes 1579382 | solution.py:24
  155.3 1.2 fusion.96
  156.6 1.2 fusion.96
  157.9 1.2 fusion.96
  159.2 1.2 fusion.96
  160.6 1.2 fusion.96
  161.9 1.2 fusion.96
  163.2 1.2 fusion.96
  164.8 0.9 fusion.68
  165.8 1.7 fusion.80
  167.6 4.4 %fusion.22 = f32[4,8,256,64]{2,3,1,0:T(8,128)S(1)} fusion(bf16[4,8,64,128]{3,2,1,0:T(8,128)(2,1)S(1)} %bitcast.229, f32[8,4,128,256]{3,2,1,0:T(8,128)} %get-tuple-element.240, f32[4,8]{0,1:T(8,128)S(1)} %fusion.73, f32[4,128,256]{2,1,0:T(8,128)S(1)} %get-tuple-element.239, f32[4,8]{0,1:T(8,128)S(1)} %get-tuple-element.432), kind=kOutput, calls=%fused_computation.45 | convolution fusion | flops 808452096 | bytes 7340288 | tf_op jit(solution)/shard_map/hctk,hckv->hctv/dot_general | solution.py:107
  172.0 2.2 multiply_reduce_fusion.2
  175.4 1.1 copy-done.4
  176.5 1.4 copy.88
  178.4 0.7 copy-done.5
  179.1 0.7 multiply_convert_fusion
  179.8 3.6 pad_maximum_fusion
  183.7 120.8 %all-gather.9.cloned.1.call-done = bf16[1536,4096]{1,0:T(8,128)(2,1)} async-done(((bf16[1536,1024]{1,0:T(8,128)(2,1)}), bf16[1536,4096]{1,0:T(8,128)(2,1)}) %all-gather.9.cloned.1.call-update) | async-done | bytes 12582928 | tf_op jit(solution)/shard_map/all_gather | solution.py:195
  304.5 5.2 %multiply_reduce_fusion = f32[1024]{0:T(1024)S(1)} fusion(bf16[1536,4096]{1,0:T(8,128)(2,1)} %all-gather.9.cloned.1.call-done), kind=kLoop, calls=%fused_computation.36 | loop fusion | flops 12581888 | bytes 8392704 | tf_op jit(solution)/shard_map/reduce_sum | solution.py:204
  309.8 5.9 %fusion.36 = f32[1024,256]{1,0:T(8,128)S(1)} fusion(bf16[1,256,4096]{2,1,0:T(8,128)(2,1)S(1)} %copy-done.10, bf16[1536,4096]{1,0:T(8,128)(2,1)} %all-gather.9.cloned.1.call-done, f32[1024]{0:T(1024)S(1)} %add_rsqrt_fusion.1), kind=kOutput, calls=%fused_computation.68 | convolution fusion | flops 2147745792 | bytes 11538432 | tf_op jit(solution)/shard_map/sd,fd->sf/dot_general | solution.py:202
  316.2 3.3 fusion.51
  319.5 35.2 %all-gather.11.cloned.1.call-done = bf16[1024,1024]{1,0:T(8,128)(2,1)} async-done(((bf16[1024,256]{1,0:T(8,128)(2,1)}), bf16[1024,1024]{1,0:T(8,128)(2,1)}) %all-gather.11.cloned.1.call-update) | async-done | bytes 2097168 | tf_op jit(solution)/shard_map/all_gather | solution.py:210
  354.7 5.3 %fusion.29 = bf16[1024,1024]{1,0:T(8,128)(2,1)} fusion(bf16[1024,1024]{1,0:T(8,128)(2,1)} %all-gather.11.cloned.1.call-done, bf16[1,1024,1024]{2,1,0:T(8,128)(2,1)S(1)} %copy-done), kind=kOutput, calls=%fused_computation.64 | convolution fusion | flops 2148532224 | bytes 6291456 | tf_op jit(solution)/shard_map/dot_general | solution.py:209
  360.0 4.7 %all-to-all-start.1 = ((bf16[8,128,1024]{2,1,0:T(8,128)(2,1)}), bf16[8,128,1024]{2,1,0:T(8,128)(2,1)}, u32[]{:S(2)}, u32[]{:S(2)}) async-start(bf16[8,128,1024]{2,1,0:T(8,128)(2,1)} %bitcast.230), calls=%async_computation.1 | async-start | bytes 4194304 | tf_op jit(solution)/shard_map/all_to_all | solution.py:214
  365.6 10.1 %fusion.32 = bf16[512,1024]{1,0:T(8,128)(2,1)} fusion(bf16[4096,1024]{1,0:T(8,128)(2,1)} %param.25, bf16[1536,4096]{1,0:T(8,128)(2,1)} %all-gather.9.cloned.1.call-done), kind=kOutput, calls=%fused_computation.65 | convolution fusion | flops 4295491584 | bytes 13631488 | tf_op jit(solution)/shard_map/dot_general | solution.py:201
  375.8 38.1 %all-to-all-done.1 = bf16[8,128,1024]{2,1,0:T(8,128)(2,1)} async-done(((bf16[8,128,1024]{2,1,0:T(8,128)(2,1)}), bf16[8,128,1024]{2,1,0:T(8,128)(2,1)}, u32[]{:S(2)}, u32[]{:S(2)}) %all-to-all-start.1) | async-done | bytes 2097184 | tf_op jit(solution)/shard_map/all_to_all | solution.py:214
  413.9 4.6 %gather_fusion.1 = bf16[512,1024]{1,0:T(8,128)(2,1)S(1)} fusion(bf16[1024,1024]{1,0:T(8,128)(2,1)} %bitcast.39, s32[1024]{0:T(1024)S(1)} %pad_clamp_fusion), kind=kCustom, calls=%fused_computation.1 | custom fusion | bytes 2099200 | tf_op jit(solution)/shard_map/jit(_take)/gather | solution.py:218
  418.5 1.2 gather.15
  419.7 6.3 %multiply_reduce_fusion.1 = bf16[256,1024]{1,0:T(8,128)(2,1)} fusion(bf16[256,2,1024]{2,1,0:T(2,128)(2,1)} %gather.15, pred[256,2]{1,0:T(8,128)(4,1)S(1)} %copy.93, f32[256,2]{1,0:T(8,128)S(1)} %copy.95), kind=kLoop, calls=%fused_computation.56 | loop fusion | flops 1835008 | bytes 1575424 | tf_op jit(solution)/shard_map/reduce_sum | solution.py:220
  (179 shorter events, 10.0 us)
Async XLA Ops:
  7.2 347.5 %copy-start = (bf16[1,1024,1024]{2,1,0:T(8,128)(2,1)S(1)}, bf16[1,1024,1024]{2,1,0:T(8,128)(2,1)}, u32[]{:S(2)}) copy-start(bf16[1,1024,1024]{2,1,0:T(8,128)(2,1)} %param.31) | copy-start | bytes 6291460
  7.2 148.0 %all-gather.13.cloned.1.call-start = ((), (), s32[]{:S(2)}) async-start(), calls=%async_computation.4 | async-start | bytes 4718592 | tf_op jit(solution)/shard_map/all_gather | solution.py:15
  22.4 18.9 %copy-start.7 = (s32[256,2]{0,1:T(2,128)S(1)}, s32[256,2]{0,1:T(2,128)}, u32[]{:S(2)}) copy-start(s32[256,2]{0,1:T(2,128)} %param.27) | copy-start | bytes 6148
  40.4 0.8 copy-start.2
  40.5 3.4 copy-start.1
  52.1 6.6 %copy-start.12 = (u32[32]{0:T(128)S(1)}, u32[32]{0:T(128)}, u32[]{:S(2)}) copy-start(u32[32]{0:T(128)} %constant.145) | copy-start | bytes 388
  52.1 79.5 %copy-start.6 = (bf16[512,512]{1,0:T(8,128)(2,1)S(1)}, bf16[512,512]{1,0:T(8,128)(2,1)}, u32[]{:S(2)}) copy-start(bf16[512,512]{1,0:T(8,128)(2,1)} %param.18) | copy-start | bytes 1572868
  52.1 127.7 %all-to-all-start = ((bf16[8,128,1024]{2,1,0:T(8,128)(2,1)}), bf16[8,128,1024]{2,1,0:T(8,128)(2,1)}, u32[]{:S(2)}, u32[]{:S(2)}) async-start(bf16[8,128,1024]{2,1,0:T(8,128)(2,1)} %select_select_fusion), calls=%async_computation | async-start | bytes 4194304 | tf_op jit(solution)/shard_map/all_to_all | solution.py:183
  58.7 245.8 %all-gather.9.cloned.1.call-start = ((), (), s32[]{:S(2)}) async-start(), calls=%async_computation.2 | async-start | bytes 15728640 | tf_op jit(solution)/shard_map/all_gather | solution.py:195
  167.5 4.4 %copy-start.3 = (bf16[4,512,256]{2,1,0:T(8,128)(2,1)S(1)}, bf16[4,512,256]{2,1,0:T(8,128)(2,1)}, u32[]{:S(2)}) copy-start(bf16[4,512,256]{2,1,0:T(8,128)(2,1)} %copy.78) | copy-start | bytes 3145732
  174.9 1.6 copy-start.4
  177.9 1.2 copy-start.5
  177.9 1.2 copy-start.8
  183.4 171.3 %all-gather.11.cloned.1.call-start = ((), (), s32[]{:S(2)}) async-start(), calls=%async_computation.3 | async-start | bytes 2621440 | tf_op jit(solution)/shard_map/all_gather | solution.py:210
  304.5 5.2 %copy-start.10 = (bf16[1,256,4096]{2,1,0:T(8,128)(2,1)S(1)}, bf16[1,256,4096]{2,1,0:T(8,128)(2,1)}, u32[]{:S(2)}) copy-start(bf16[1,256,4096]{2,1,0:T(8,128)(2,1)} %param.29) | copy-start | bytes 6291460
  304.5 11.2 %slice-start = ((s8[12582912]{0:T(1024)(128)(4,1)}), s8[4194304]{0:T(1024)(128)(4,1)S(1)}, s32[]{:S(2)}) async-start(s8[12582912]{0:T(1024)(128)(4,1)} %bitcast.220), calls=%async_computation.5 | async-start | bytes 8388608
  309.7 6.0 %slice-start.1 = ((s8[12582912]{0:T(1024)(128)(4,1)}), s8[4194304]{0:T(1024)(128)(4,1)S(1)}, s32[]{:S(2)}) async-start(s8[12582912]{0:T(1024)(128)(4,1)} %bitcast.220), calls=%async_computation.6 | async-start | bytes 8388608
  309.7 6.5 %slice-start.2 = ((s8[12582912]{0:T(1024)(128)(4,1)}), s8[4194304]{0:T(1024)(128)(4,1)S(1)}, s32[]{:S(2)}) async-start(s8[12582912]{0:T(1024)(128)(4,1)} %bitcast.220), calls=%async_computation.7 | async-start | bytes 8388608
  309.7 6.5 %copy-start.11 = (bf16[1,256,4096]{2,1,0:T(8,128)(2,1)S(1)}, bf16[1,256,4096]{2,1,0:T(8,128)(2,1)}, u32[]{:S(2)}) copy-start(bf16[1,256,4096]{2,1,0:T(8,128)(2,1)} %param.30) | copy-start | bytes 6291460
  360.0 5.5 %copy-start.9 = (f32[256,2]{0,1:T(2,128)S(1)}, f32[256,2]{0,1:T(2,128)}, u32[]{:S(2)}) copy-start(f32[256,2]{0,1:T(2,128)} %param.28) | copy-start | bytes 6148
  360.0 53.9 %all-to-all-start.1 = ((bf16[8,128,1024]{2,1,0:T(8,128)(2,1)}), bf16[8,128,1024]{2,1,0:T(8,128)(2,1)}, u32[]{:S(2)}, u32[]{:S(2)}) async-start(bf16[8,128,1024]{2,1,0:T(8,128)(2,1)} %bitcast.230), calls=%async_computation.1 | async-start | bytes 4194304 | tf_op jit(solution)/shard_map/all_to_all | solution.py:214
Sparse Core Ops, SparseCore 0:
  41.4 85.6 all-gather.12
  183.5 120.9 all-gather.8
  319.6 35.0 all-gather.10
